TPU v7x, 32 devices: a whole 2x2x4 slice. The times are simulated.
32 devices in a mesh: kv: 16 (over z, y, x), tp: 2 (over core).
Axes of the slice: x: 2, y: 2, z: 4, core: 2. Of those that a mesh axis runs over, the one named last changes fastest.
Arguments:
- tokens: bfloat16 [160, 3, 2048], P('kv', None, 'tp'), may hold values from -6 to 6
- norm_gain: float32 [2048], replicated, may hold values from 0.1 to 1.9
- w_query: bfloat16 [2048, 1024], P('kv', 'tp'), may hold values from -0.125 to 0.125
- w_key: bfloat16 [2048, 1024], P('kv', 'tp'), may hold values from -0.125 to 0.125
- w_value: bfloat16 [2048, 2048], P('kv', 'tp'), may hold values from -0.125 to 0.125
- w_igate: bfloat16 [2048, 8], replicated, may hold values from -0.125 to 0.125
- w_fgate: bfloat16 [2048, 8], replicated, may hold values from -0.125 to 0.125
- igate_bias: float32 [8], replicated, may hold values from -5 to -2
- fgate_bias: float32 [8], replicated, may hold values from 0.5 to 4
- prev_keys: bfloat16 [160, 3, 1024], P('kv', None, 'tp'), may hold values from -6 to 6
- prev_values: bfloat16 [160, 3, 2048], P('kv', None, 'tp'), may hold values from -6 to 6
- prev_igate: float32 [160, 3, 8], P('kv', None, 'tp'), may hold values from -4 to 0
- prev_logf: float32 [160, 3, 8], P('kv', None, 'tp'), may hold values from -0.6 to -0.02
- accepted: int32 [160], P('kv'), may hold values from 0 to 3
- state_mem: float32 [160, 8, 128, 256], P('kv', 'tp'), may hold values from -2 to 2
- state_norm: float32 [160, 8, 128], P('kv', 'tp'), may hold values from -2 to 2
- state_max: float32 [160, 8], P('kv', 'tp'), may hold values from -3 to 0
Outputs:
- readout: bfloat16 [160, 3, 2048], P('kv', None, 'tp')
- base_mem: float32 [160, 8, 128, 256], P('kv', 'tp')
- base_norm: float32 [160, 8, 128], P('kv', 'tp')
- base_max: float32 [160, 8], P('kv', 'tp')
Inputs may be any that keep to these rules, and one draw needn't show every extreme that they name: Proposal j of a sequence is live when j < accepted of that sequence.
All inputs are finite; a program needn't handle non-finite values.
Results may differ from a plain program's by a relative error of at most 0.0073.
Values may be sent and summed in bfloat16 or wider, within the bound.
A program may use at most 64 MiB of HBM per device.

v0:
```python
import functools

import jax
import jax.numpy as jnp
from jax import lax
from jax.experimental import pallas as pl
from jax.experimental.pallas import tpu as pltpu
from jax.sharding import PartitionSpec as P

epsilon = 1e-06
highest = lax.Precision.HIGHEST


def base_kernel(
    keys_ref,
    values_ref,
    gate_ref,
    logf_ref,
    accepted_ref,
    mem_ref,
    norm_ref,
    max_ref,
    mem_out,
    norm_out,
    max_out,
    weights,
):
    step = pl.program_id(0)
    length = gate_ref.shape[0]
    heads, seqs = max_ref.shape
    key_width, value_width = mem_ref.shape[2:]
    key_scale = key_width ** (-0.5)

    @pl.when(step == 0)
    def _():
        accepted = accepted_ref[...]
        running = jnp.zeros((heads, seqs), jnp.float32)
        sums = []
        for j in range(length):
            running = running + jnp.where(j < accepted, logf_ref[j], 0.0)
            sums.append(running)
        logs = [
            jnp.where(j < accepted, running - sums[j] + gate_ref[j], -jnp.inf)
            for j in range(length)
        ]
        base_max = running + max_ref[...]
        for log in logs:
            base_max = jnp.maximum(base_max, log)
        max_out[...] = base_max
        for j in range(length):
            weights[j] = jnp.exp(logs[j] - base_max)
        weights[length] = jnp.exp(running + max_ref[...] - base_max)

    here = lax.broadcasted_iota(jnp.int32, (heads, seqs), 1) == step
    picked = [
        jnp.sum(jnp.where(here, weights[j], 0.0), axis=1, keepdims=True) for j in range(length + 1)
    ]
    keys = keys_ref[0].astype(jnp.float32) * key_scale
    values = values_ref[0]
    for h in range(heads):
        cols = keys[:, h * key_width : (h + 1) * key_width]
        scaled = jnp.concatenate(
            [cols[j : j + 1] * picked[j][h : h + 1] for j in range(length)], axis=0
        )
        high = scaled.astype(jnp.bfloat16).astype(jnp.float32)
        low = scaled - high
        left = jnp.concatenate([high, low], axis=0).astype(jnp.bfloat16)
        mine = values[:, h * value_width : (h + 1) * value_width].astype(jnp.float32)
        right = jnp.concatenate([mine, mine], axis=0).astype(jnp.bfloat16)
        update = lax.dot_general(
            left, right, (((0,), (0,)), ((), ())), preferred_element_type=jnp.float32
        )
        carry = picked[length][h : h + 1]
        mem_out[0, h] = carry * mem_ref[0, h] + update
        norm_out[0, h : h + 1] = carry * norm_ref[0, h : h + 1] + jnp.sum(
            scaled, axis=0, keepdims=True
        )


def fold_accepted(
    prev_keys, prev_values, prev_igate, prev_logf, accepted, state_mem, state_norm, state_max
):
    seqs, heads, key_width, value_width = state_mem.shape
    length = prev_keys.shape[1]

    def per_seq(*shape):
        return pl.BlockSpec((1,) + shape, lambda i: (i,) + (0,) * len(shape))

    def whole(*shape):
        return pl.BlockSpec(shape, lambda i: (0,) * len(shape))

    base_mem, base_norm, base_max = pl.pallas_call(
        base_kernel,
        grid=(seqs,),
        out_shape=(
            jax.ShapeDtypeStruct(state_mem.shape, jnp.float32),
            jax.ShapeDtypeStruct(state_norm.shape, jnp.float32),
            jax.ShapeDtypeStruct((heads, seqs), jnp.float32),
        ),
        in_specs=[
            per_seq(length, prev_keys.shape[2]),
            per_seq(length, prev_values.shape[2]),
            whole(length, heads, seqs),
            whole(length, heads, seqs),
            whole(1, seqs),
            per_seq(heads, key_width, value_width),
            per_seq(heads, key_width),
            whole(heads, seqs),
        ],
        out_specs=(
            per_seq(heads, key_width, value_width),
            per_seq(heads, key_width),
            whole(heads, seqs),
        ),
        scratch_shapes=[pltpu.VMEM((length + 1, heads, seqs), jnp.float32)],
        name="base",
    )(
        prev_keys,
        prev_values,
        prev_igate.transpose(1, 2, 0),
        prev_logf.transpose(1, 2, 0),
        accepted.reshape(1, -1),
        state_mem,
        state_norm,
        state_max.T,
    )
    return base_mem, base_norm, base_max


def factor(count):
    inner = 1
    while inner * inner * 4 <= count and count % (inner * 2) == 0:
        inner *= 2
    return count // inner, inner


def project_kernel(
    reduce_n,
    outer_n,
    inner_n,
    tp_n,
    tok_ref,
    gain_ref,
    wq_ref,
    wk_ref,
    wv_ref,
    wi_ref,
    wf_ref,
    bi_ref,
    bf_ref,
    mem_ref,
    norm_ref,
    max_ref,
    out_ref,
    xfull,
    xrows,
    memv,
    mem16,
    carried,
    nbuf,
    abuf,
    xall,
    wbuf,
    pbuf,
    own,
    sbuf,
    rbuf,
    tok_local,
    tok_send,
    tok_recv,
    a_send,
    a_recv,
    w_local,
    w_send,
    w_recv,
    fy_send,
    fx_send,
    fy_recv,
    fx_recv,
    p_send,
    p_recv,
    mem_sem,
):
    group_n = outer_n * inner_n
    chunks, rows_all, width = wbuf.shape
    depth = rows_all // group_n
    half = depth // 2
    seqs, length, part = tok_ref.shape
    rows = seqs * length
    heads, _, value_width = mem16.shape
    key_width = mem_ref.shape[2]
    key_scale = key_width ** (-0.5)
    stride = xall.shape[0] // reduce_n
    block = nbuf.shape[2]

    kv = lax.axis_index("kv")
    tp = lax.axis_index("tp")
    red, grp = kv // group_n, kv % group_n
    outer, inner = grp // inner_n, grp % inner_n

    def at_grp(index):
        return {"kv": red * group_n + index}

    x_peers = [outer * inner_n + (inner + d) % inner_n for d in range(1, inner_n)]
    y_peers = [((outer + d) % outer_n) * inner_n + inner for d in range(1, outer_n)]
    r_peers = [(red + d) % reduce_n for d in range(1, reduce_n)]
    t_peers = [(tp + d) % tp_n for d in range(1, tp_n)]

    barrier = pltpu.get_barrier_semaphore()
    targets = (
        [{"tp": t} for t in t_peers]
        + [at_grp(p) for p in x_peers + y_peers]
        + [{"kv": p * group_n + grp} for p in r_peers]
    )
    for target in targets:
        pl.semaphore_signal(barrier, inc=1, device_id=target, device_id_type=pl.DeviceIdType.MESH)

    def chunk_of(c):
        if c == 0:
            return wq_ref
        if c == 1:
            return wk_ref
        return wv_ref.at[:, pl.ds((c - 2) * width, width)]

    def slot(c, source, start=0, size=None):
        size = depth if size is None else size
        first = pl.multiple_of(source * depth + start, half)
        return wbuf.at[c, pl.ds(first, size), :]

    def remote(src, dst, send, recv, target):
        return pltpu.make_async_remote_copy(
            src_ref=src,
            dst_ref=dst,
            send_sem=send,
            recv_sem=recv,
            device_id=target,
            device_id_type=pl.DeviceIdType.MESH,
        )

    locals_ = [pltpu.make_async_copy(tok_ref, xfull.at[tp], tok_local)]
    for c in range(chunks):
        locals_.append(pltpu.make_async_copy(chunk_of(c), slot(c, grp), w_local.at[c]))
    for copy in locals_:
        copy.start()
    mem_copy = pltpu.make_async_copy(mem_ref, memv, mem_sem)
    mem_copy.start()
    pl.semaphore_wait(barrier, len(targets))

    sends = []

    def go(copy):
        copy.start()
        sends.append(copy)

    for i, t in enumerate(t_peers):
        go(remote(tok_ref, xfull.at[tp], tok_send.at[i], tok_recv.at[tp], {"tp": t}))

    def direct(c):
        for i, p in enumerate(x_peers + y_peers):
            go(remote(chunk_of(c), slot(c, grp), w_send.at[c, i], w_recv.at[c, grp], at_grp(p)))

    direct(0)
    if chunks > 1:
        direct(1)

    for copy in locals_:
        copy.wait()
    for t in t_peers:
        remote(tok_ref, xfull.at[t], tok_send.at[0], tok_recv.at[t], {"tp": t}).wait_recv()

    total = jnp.zeros((rows, 1), jnp.float32)
    for t in range(tp_n):
        for n in range(seqs):
            xrows[t, n * length : (n + 1) * length] = xfull[t, n].astype(jnp.float32)
        piece = xrows[t]
        total = total + jnp.sum(piece * piece, axis=1, keepdims=True)
    factor_rows = lax.rsqrt(total / (tp_n * part) + epsilon)
    step = min(block, part)
    for p in range(reduce_n * block // step):
        first = p * step
        piece = xrows[first // part, :, first % part : first % part + step]
        normed = (piece * factor_rows * gain_ref[:, first : first + step]).astype(jnp.bfloat16)
        nbuf[first // block, :, first % block : first % block + step] = normed

    for i, p in enumerate(r_peers):
        go(remote(nbuf.at[p], abuf.at[red], a_send.at[i], a_recv.at[red], {"kv": p * group_n + grp}))
    abuf[red] = nbuf[red]

    dims = (((1,), (1,)), ((), ()))
    gate_i = jnp.zeros((rows, wi_ref.shape[0]), jnp.float32)
    gate_f = jnp.zeros((rows, wf_ref.shape[0]), jnp.float32)
    for p in range(reduce_n):
        cols = slice(p * block, (p + 1) * block)
        piece = nbuf[p]
        gate_i += lax.dot_general(piece, wi_ref[:, cols], dims, preferred_element_type=jnp.float32)
        gate_f += lax.dot_general(piece, wf_ref[:, cols], dims, preferred_element_type=jnp.float32)
    gate_i = gate_i + bi_ref[...]
    gate_f = jax.nn.log_sigmoid(gate_f + bf_ref[...])
    row_id = lax.broadcasted_iota(jnp.int32, (rows, rows), 0)
    col_id = lax.broadcasted_iota(jnp.int32, (rows, rows), 1)
    causal = (row_id // length == col_id // length) & (col_id <= row_id)
    same = row_id == col_id
    belongs = (
        lax.broadcasted_iota(jnp.int32, (rows, seqs), 0) // length
        == lax.broadcasted_iota(jnp.int32, (rows, seqs), 1)
    )
    head_id = lax.broadcasted_iota(jnp.int32, gate_i.shape, 1)

    def turned(column):
        return jnp.sum(jnp.where(same, column, 0.0), axis=0, keepdims=True)

    decays, tops, carries = [], [], []
    for h in range(heads):
        chosen = head_id == tp * heads + h
        in_gate = jnp.sum(jnp.where(chosen, gate_i, 0.0), axis=1, keepdims=True)
        log_forget = jnp.sum(jnp.where(chosen, gate_f, 0.0), axis=1, keepdims=True)
        running = jnp.sum(jnp.where(causal, turned(log_forget), 0.0), axis=1, keepdims=True)
        within = jnp.where(causal, running + turned(in_gate - running), -jnp.inf)
        base_max = jnp.sum(jnp.where(belongs, max_ref[h : h + 1], 0.0), axis=1, keepdims=True)
        top = jnp.maximum(running + base_max, jnp.max(within, axis=1, keepdims=True))
        decays.append(jnp.exp(within - top) * key_scale)
        carries.append(jnp.exp(running + base_max - top))
        tops.append(jnp.exp(-top))

    xall[...] = jnp.zeros_like(xall)
    for p in r_peers:
        remote(nbuf.at[p], abuf.at[p], a_send.at[0], a_recv.at[p], {"kv": p * group_n + grp}).wait_recv()
    for p in range(reduce_n):
        xall[p * stride : p * stride + rows, :] = abuf[p]

    def relay(c):
        for i, p in enumerate(x_peers):
            remote(chunk_of(c), slot(c, p), w_send.at[c, 0], w_recv.at[c, p], at_grp(p)).wait_recv()
            for j, q in enumerate(y_peers):
                go(
                    remote(
                        slot(c, p, 0, half),
                        slot(c, p, 0, half),
                        fy_send.at[c, i, j],
                        fy_recv.at[c, p],
                        at_grp(q),
                    )
                )
        for j, q in enumerate(y_peers):
            remote(chunk_of(c), slot(c, q), w_send.at[c, 0], w_recv.at[c, q], at_grp(q)).wait_recv()
            for i, p in enumerate(x_peers):
                go(
                    remote(
                        slot(c, q, half, half),
                        slot(c, q, half, half),
                        fx_send.at[c, i, j],
                        fx_recv.at[c, q],
                        at_grp(p),
                    )
                )
        if c + 2 < chunks:
            direct(c + 2)

    def partial(c):
        for i in range(1, inner_n):
            for j in range(1, outer_n):
                source = ((outer + j) % outer_n) * inner_n + (inner + i) % inner_n
                for start, send, recv in ((0, fy_send, fy_recv), (half, fx_send, fx_recv)):
                    here = slot(c, source, start, half)
                    remote(here, here, send.at[c, 0, 0], recv.at[c, source], at_grp(source)).wait_recv()
        product = jnp.dot(xall[...], wbuf[c], preferred_element_type=jnp.float32)
        for p in range(reduce_n):
            piece = product[p * stride : p * stride + rows]
            pbuf[p] = piece
            sbuf[c, p] = piece.astype(jnp.bfloat16)
        own[c] = pbuf[red]
        for i, p in enumerate(r_peers):
            go(
                remote(
                    sbuf.at[c, p],
                    rbuf.at[c, red],
                    p_send.at[c, i],
                    p_recv.at[c, red],
                    {"kv": p * group_n + grp},
                )
            )

    def settle(c):
        total = own[c]
        for p in r_peers:
            remote(
                sbuf.at[c, p], rbuf.at[c, p], p_send.at[c, 0], p_recv.at[c, p], {"kv": p * group_n + grp}
            ).wait_recv()
            total = total + rbuf[c, p].astype(jnp.float32)
        return total.astype(jnp.bfloat16)

    kept = {}

    def finish(c):
        done = settle(c)
        if c == 0:
            kept["query"] = done
            seq_id = lax.broadcasted_iota(jnp.int32, (rows, key_width), 0) // length
            for h in range(heads):
                query = done[:, h * key_width : (h + 1) * key_width].astype(jnp.float32)
                spread = jnp.concatenate(
                    [jnp.where(seq_id == n, query, 0.0).astype(jnp.bfloat16) for n in range(seqs)],
                    axis=1,
                )
                held = jnp.dot(spread, mem16[h], preferred_element_type=jnp.float32)
                carried[h] = held * carries[h]
                against = lax.dot_general(
                    query, norm_ref[:, h, :], dims, precision=highest,
                    preferred_element_type=jnp.float32,
                )
                kept["norm", h] = carries[h] * jnp.sum(
                    jnp.where(belongs, against, 0.0), axis=1, keepdims=True
                )
        elif c == 1:
            for h in range(heads):
                cols = slice(h * key_width, (h + 1) * key_width)
                scores = decays[h] * lax.dot_general(
                    kept["query"][:, cols], done[:, cols], dims, preferred_element_type=jnp.float32
                )
                den = jnp.sum(scores, axis=1, keepdims=True) + kept["norm", h]
                kept["scores", h] = scores
                kept["den", h] = jnp.maximum(jnp.abs(den), tops[h])
        else:
            wide = min(width, value_width)
            for i in range(width // wide):
                first = (c - 2) * width + i * wide
                h, sub = first // value_width, first % value_width
                scores = kept["scores", h]
                high = scores.astype(jnp.bfloat16)
                low = (scores - high.astype(jnp.float32)).astype(jnp.bfloat16)
                mine = done[:, i * wide : (i + 1) * wide]
                num = carried[h, :, sub : sub + wide]
                num = num + jnp.dot(high, mine, preferred_element_type=jnp.float32)
                num = num + jnp.dot(low, mine, preferred_element_type=jnp.float32)
                result = num / kept["den", h]
                for n in range(seqs):
                    out_ref[n, :, first : first + wide] = result[
                        n * length : (n + 1) * length
                    ].astype(jnp.bfloat16)

    for c in range(chunks + 2):
        if c < chunks:
            relay(c)
            if c == 0:
                mem_copy.wait()
            for h in range(c, heads, 2) if c < 2 else ():
                mem16[h] = memv[:, h].reshape(seqs * key_width, value_width).astype(jnp.bfloat16)
        if 1 <= c <= chunks:
            partial(c - 1)
        if c >= 2:
            finish(c - 2)
    for copy in sends:
        copy.wait_send()


def project(
    tokens,
    norm_gain,
    w_query,
    w_key,
    w_value,
    w_igate,
    w_fgate,
    igate_bias,
    fgate_bias,
    base_mem,
    base_norm,
    base_max,
    kv_n,
    tp_n,
):
    seqs, length, part = tokens.shape
    rows = seqs * length
    heads, key_width, value_width = base_mem.shape[1:]
    depth, width = w_query.shape
    chunks = 2 + w_value.shape[1] // width
    reduce_n, group_n = factor(kv_n)
    outer_n, inner_n = factor(group_n)
    block = group_n * depth
    stride = -(-rows // 16) * 16
    dma = pltpu.SemaphoreType.DMA
    peers = max(1, outer_n + inner_n - 2)
    vmem = pl.BlockSpec(memory_space=pltpu.VMEM)
    return pl.pallas_call(
        functools.partial(project_kernel, reduce_n, outer_n, inner_n, tp_n),
        out_shape=jax.ShapeDtypeStruct((seqs, length, heads * value_width), jnp.bfloat16),
        in_specs=[vmem] * 9 + [pl.BlockSpec(memory_space=pl.ANY), vmem, vmem],
        out_specs=vmem,
        scratch_shapes=[
            pltpu.VMEM((tp_n, seqs, length, part), jnp.bfloat16),
            pltpu.VMEM((tp_n, rows, part), jnp.float32),
            pltpu.VMEM(base_mem.shape, jnp.float32),
            pltpu.VMEM((heads, seqs * key_width, value_width), jnp.bfloat16),
            pltpu.VMEM((heads, rows, value_width), jnp.float32),
            pltpu.VMEM((reduce_n, rows, block), jnp.bfloat16),
            pltpu.VMEM((reduce_n, rows, block), jnp.bfloat16),
            pltpu.VMEM((reduce_n * stride, block), jnp.bfloat16),
            pltpu.VMEM((chunks, block, width), jnp.bfloat16),
            pltpu.VMEM((reduce_n, rows, width), jnp.float32),
            pltpu.VMEM((chunks, rows, width), jnp.float32),
            pltpu.VMEM((chunks, reduce_n, rows, width), jnp.bfloat16),
            pltpu.VMEM((chunks, reduce_n, rows, width), jnp.bfloat16),
            dma,
            dma((tp_n,)),
            dma((tp_n,)),
            dma((reduce_n,)),
            dma((reduce_n,)),
            dma((chunks,)),
            dma((chunks, peers)),
            dma((chunks, group_n)),
            dma((chunks, inner_n, outer_n)),
            dma((chunks, inner_n, outer_n)),
            dma((chunks, group_n)),
            dma((chunks, group_n)),
            dma((chunks, reduce_n)),
            dma((chunks, reduce_n)),
            dma,
        ],
        compiler_params=pltpu.CompilerParams(collective_id=0, has_side_effects=True),
        name="project",
    )(
        tokens,
        norm_gain.reshape(1, -1),
        w_query,
        w_key,
        w_value,
        w_igate.T,
        w_fgate.T,
        igate_bias.reshape(1, -1),
        fgate_bias.reshape(1, -1),
        base_mem,
        base_norm,
        base_max,
    )


def shards(
    kv_n,
    tp_n,
    tokens,
    norm_gain,
    w_query,
    w_key,
    w_value,
    w_igate,
    w_fgate,
    igate_bias,
    fgate_bias,
    prev_keys,
    prev_values,
    prev_igate,
    prev_logf,
    accepted,
    state_mem,
    state_norm,
    state_max,
):
    base_mem, base_norm, base_max = fold_accepted(
        prev_keys, prev_values, prev_igate, prev_logf, accepted, state_mem, state_norm, state_max
    )
    readout = project(
        tokens,
        norm_gain,
        w_query,
        w_key,
        w_value,
        w_igate,
        w_fgate,
        igate_bias,
        fgate_bias,
        base_mem,
        base_norm,
        base_max,
        kv_n,
        tp_n,
    )
    return (readout, base_mem, base_norm, base_max.T)


def solution(mesh):
    return jax.shard_map(
        functools.partial(shards, mesh.shape["kv"], mesh.shape["tp"]),
        mesh=mesh,
        in_specs=(
            P("kv", None, "tp"),
            P(),
            P("kv", "tp"),
            P("kv", "tp"),
            P("kv", "tp"),
            P(),
            P(),
            P(),
            P(),
            P("kv", None, "tp"),
            P("kv", None, "tp"),
            P("kv", None, "tp"),
            P("kv", None, "tp"),
            P("kv"),
            P("kv", "tp", None, None),
            P("kv", "tp", None),
            P("kv", "tp"),
        ),
        out_specs=(
            P("kv", None, "tp"),
            P("kv", "tp", None, None),
            P("kv", "tp", None),
            P("kv", "tp"),
        ),
        check_vma=False,
    )
```

profile of v0, /device:TPU:0, one launch (start us, length us, event | category | flops | bytes accessed | tf_op | source)
XLA Modules:
  0.0 45.1 jit_solution(11935911320952164102)
XLA Ops:
  0.6 9.5 %base.1 = (f32[10,4,128,256]{3,2,1,0:T(8,128)}, f32[10,4,128]{2,1,0:T(4,128)}, f32[4,10]{1,0:T(4,128)}) custom-call(bf16[10,3,512]{2,1,0:T(4,128)(2,1)} %keys_ref.1, bf16[10,3,1024]{2,1,0:T(4,128)(2,1)} %values_ref.1, f32[3,4,10]{2,1,0:T(4,128)} %bitcast.13, f32[3,4,10]{2,1,0:T(4,128)} %bitcast.14, s32[1,10]{1,0:T(1,128)} %bitcast.17, ...), custom_call_target="tpu_custom_call" | custom-call | tf_op jit(solution)/shard_map/base/pallas_call | solution.py:92
  10.1 33.4 %project.1 = bf16[10,3,1024]{2,1,0:T(4,128)(2,1)} custom-call(bf16[10,3,1024]{2,1,0:T(4,128)(2,1)} %tok_ref.1, f32[1,2048]{1,0:T(1,128)} %bitcast.12, bf16[128,512]{1,0:T(8,128)(2,1)} %wq_ref.1, bf16[128,512]{1,0:T(8,128)(2,1)} %wk_ref.1, bf16[128,1024]{1,0:T(8,128)(2,1)} %wv_ref.1, bf16[8,2048]{1,0:T(8,128)(2,1)} %bitcast.10, bf16[8,2048]{1,0:T(8,128)(2,1)} %bitcast.11, ...), custom_call_target="tpu_custom_call" | custom-call | tf_op jit(solution)/shard_map/project/pallas_call | solution.py:484
  43.5 1.6 %copy.22 = bf16[10,3,1024]{2,1,0:T(4,128)(2,1)} copy(bf16[10,3,1024]{2,1,0:T(4,128)(2,1)} %project.1) | data formatting | bytes 122880
where the time goes:
time: 45.5 us; the launch traced here: 45.1 us
  Pallas kernels  42.9 us (94%)
  local copies, waits for them, and re-layouts  1.55 us (3%)
  between operations  0.64 us (1%)
    pallas_call x1, Pallas kernels, project(): pl.pallas_call(functools.partial(project_kernel, reduce_n, outer_n, inner...  33.4 us
    pallas_call x1, Pallas kernels, fold_accepted(): pl.pallas_call(base_kernel, grid=(seqs,), out_shape=(jax.ShapeDtypeStruct...  9.47 us
    unnamed x1, local copies, waits for them, and re-layouts  1.55 us

commit v1 on v0

--- a/solution.py
+++ b/solution.py
@@ -11,122 +11,6 @@
 highest = lax.Precision.HIGHEST
 
 
-def base_kernel(
-    keys_ref,
-    values_ref,
-    gate_ref,
-    logf_ref,
-    accepted_ref,
-    mem_ref,
-    norm_ref,
-    max_ref,
-    mem_out,
-    norm_out,
-    max_out,
-    weights,
-):
-    step = pl.program_id(0)
-    length = gate_ref.shape[0]
-    heads, seqs = max_ref.shape
-    key_width, value_width = mem_ref.shape[2:]
-    key_scale = key_width ** (-0.5)
-
-    @pl.when(step == 0)
-    def _():
-        accepted = accepted_ref[...]
-        running = jnp.zeros((heads, seqs), jnp.float32)
-        sums = []
-        for j in range(length):
-            running = running + jnp.where(j < accepted, logf_ref[j], 0.0)
-            sums.append(running)
-        logs = [
-            jnp.where(j < accepted, running - sums[j] + gate_ref[j], -jnp.inf)
-            for j in range(length)
-        ]
-        base_max = running + max_ref[...]
-        for log in logs:
-            base_max = jnp.maximum(base_max, log)
-        max_out[...] = base_max
-        for j in range(length):
-            weights[j] = jnp.exp(logs[j] - base_max)
-        weights[length] = jnp.exp(running + max_ref[...] - base_max)
-
-    here = lax.broadcasted_iota(jnp.int32, (heads, seqs), 1) == step
-    picked = [
-        jnp.sum(jnp.where(here, weights[j], 0.0), axis=1, keepdims=True) for j in range(length + 1)
-    ]
-    keys = keys_ref[0].astype(jnp.float32) * key_scale
-    values = values_ref[0]
-    for h in range(heads):
-        cols = keys[:, h * key_width : (h + 1) * key_width]
-        scaled = jnp.concatenate(
-            [cols[j : j + 1] * picked[j][h : h + 1] for j in range(length)], axis=0
-        )
-        high = scaled.astype(jnp.bfloat16).astype(jnp.float32)
-        low = scaled - high
-        left = jnp.concatenate([high, low], axis=0).astype(jnp.bfloat16)
-        mine = values[:, h * value_width : (h + 1) * value_width].astype(jnp.float32)
-        right = jnp.concatenate([mine, mine], axis=0).astype(jnp.bfloat16)
-        update = lax.dot_general(
-            left, right, (((0,), (0,)), ((), ())), preferred_element_type=jnp.float32
-        )
-        carry = picked[length][h : h + 1]
-        mem_out[0, h] = carry * mem_ref[0, h] + update
-        norm_out[0, h : h + 1] = carry * norm_ref[0, h : h + 1] + jnp.sum(
-            scaled, axis=0, keepdims=True
-        )
-
-
-def fold_accepted(
-    prev_keys, prev_values, prev_igate, prev_logf, accepted, state_mem, state_norm, state_max
-):
-    seqs, heads, key_width, value_width = state_mem.shape
-    length = prev_keys.shape[1]
-
-    def per_seq(*shape):
-        return pl.BlockSpec((1,) + shape, lambda i: (i,) + (0,) * len(shape))
-
-    def whole(*shape):
-        return pl.BlockSpec(shape, lambda i: (0,) * len(shape))
-
-    base_mem, base_norm, base_max = pl.pallas_call(
-        base_kernel,
-        grid=(seqs,),
-        out_shape=(
-            jax.ShapeDtypeStruct(state_mem.shape, jnp.float32),
-            jax.ShapeDtypeStruct(state_norm.shape, jnp.float32),
-            jax.ShapeDtypeStruct((heads, seqs), jnp.float32),
-        ),
-        in_specs=[
-            per_seq(length, prev_keys.shape[2]),
-            per_seq(length, prev_values.shape[2]),
-            whole(length, heads, seqs),
-            whole(length, heads, seqs),
-            whole(1, seqs),
-            per_seq(heads, key_width, value_width),
-            per_seq(heads, key_width),
-            whole(heads, seqs),
-        ],
-        out_specs=(
-            per_seq(heads, key_width, value_width),
-            per_seq(heads, key_width),
-            whole(heads, seqs),
-        ),
-        scratch_shapes=[pltpu.VMEM((length + 1, heads, seqs), jnp.float32)],
-        name="base",
-    )(
-        prev_keys,
-        prev_values,
-        prev_igate.transpose(1, 2, 0),
-        prev_logf.transpose(1, 2, 0),
-        accepted.reshape(1, -1),
-        state_mem,
-        state_norm,
-        state_max.T,
-    )
-    return base_mem, base_norm, base_max
-
-
 def factor(count):
     inner = 1
     while inner * inner * 4 <= count and count % (inner * 2) == 0:
@@ -134,53 +18,69 @@
     return count // inner, inner
 
 
-def project_kernel(
+def step_kernel(
     reduce_n,
     outer_n,
     inner_n,
     tp_n,
     tok_ref,
-    gain_ref,
     wq_ref,
     wk_ref,
     wv_ref,
-    wi_ref,
-    wf_ref,
-    bi_ref,
-    bf_ref,
     mem_ref,
-    norm_ref,
-    max_ref,
-    out_ref,
-    xfull,
-    xrows,
-    memv,
-    mem16,
-    carried,
-    nbuf,
-    abuf,
-    xall,
-    wbuf,
-    pbuf,
-    own,
-    sbuf,
-    rbuf,
-    tok_local,
-    tok_send,
-    tok_recv,
-    a_send,
-    a_recv,
-    w_local,
-    w_send,
-    w_recv,
-    fy_send,
-    fx_send,
-    fy_recv,
-    fx_recv,
-    p_send,
-    p_recv,
-    mem_sem,
+    *refs,
 ):
+    small_n = 12
+    hbm_small, refs = refs[:small_n], refs[small_n:]
+    (out_ref, mem_out, norm_out, max_out), refs = refs[:4], refs[4:]
+    vmem_small, refs = refs[:small_n], refs[small_n:]
+    (
+        gain_ref,
+        wi_ref,
+        wf_ref,
+        bi_ref,
+        bf_ref,
+        keys_ref,
+        values_ref,
+        gate_ref,
+        logf_ref,
+        accepted_ref,
+        norm_ref,
+        max_ref,
+    ) = vmem_small
+    (
+        xfull,
+        xrows,
+        krows,
+        vrows,
+        scaled,
+        mem16,
+        carried,
+        nbuf,
+        abuf,
+        xall,
+        wbuf,
+        pbuf,
+        own,
+        sbuf,
+        rbuf,
+        tok_local,
+        tok_send,
+        tok_recv,
+        a_send,
+        a_recv,
+        w_local,
+        w_send,
+        w_recv,
+        fy_send,
+        fx_send,
+        fy_recv,
+        fx_recv,
+        p_send,
+        p_recv,
+        mem_sem,
+        small_sem,
+    ) = refs
     group_n = outer_n * inner_n
     chunks, rows_all, width = wbuf.shape
     depth = rows_all // group_n
@@ -242,8 +142,16 @@
         locals_.append(pltpu.make_async_copy(chunk_of(c), slot(c, grp), w_local.at[c]))
     for copy in locals_:
         copy.start()
-    mem_copy = pltpu.make_async_copy(mem_ref, memv, mem_sem)
+    small = [
+        pltpu.make_async_copy(src, dst, small_sem.at[i])
+        for i, (src, dst) in enumerate(zip(hbm_small, vmem_small))
+    ]
+    for copy in small:
+        copy.start()
+    mem_copy = pltpu.make_async_copy(mem_ref, mem_out, mem_sem)
     mem_copy.start()
+    for copy in locals_:
+        copy.wait()
     pl.semaphore_wait(barrier, len(targets))
 
     sends = []
@@ -253,18 +161,78 @@
         sends.append(copy)
 
     for i, t in enumerate(t_peers):
-        go(remote(tok_ref, xfull.at[tp], tok_send.at[i], tok_recv.at[tp], {"tp": t}))
+        go(remote(xfull.at[tp], xfull.at[tp], tok_send.at[i], tok_recv.at[tp], {"tp": t}))
 
     def direct(c):
         for i, p in enumerate(x_peers + y_peers):
-            go(remote(chunk_of(c), slot(c, grp), w_send.at[c, i], w_recv.at[c, grp], at_grp(p)))
+            go(remote(slot(c, grp), slot(c, grp), w_send.at[c, i], w_recv.at[c, grp], at_grp(p)))
 
     direct(0)
     if chunks > 1:
         direct(1)
 
-    for copy in locals_:
+    for copy in small:
         copy.wait()
+
+    row_seq = lax.broadcasted_iota(jnp.int32, (rows, seqs), 0) // length
+    row_pos = lax.broadcasted_iota(jnp.int32, (rows, seqs), 0) % length
+    belongs = row_seq == lax.broadcasted_iota(jnp.int32, (rows, seqs), 1)
+    diagonal = lax.broadcasted_iota(jnp.int32, (seqs, seqs), 0) == lax.broadcasted_iota(
+        jnp.int32, (seqs, seqs), 1
+    )
+
+    accepted = accepted_ref[...]
+    summed = jnp.zeros((heads, seqs), jnp.float32)
+    sums = []
+    for j in range(length):
+        summed = summed + jnp.where(j < accepted, logf_ref[j], 0.0)
+        sums.append(summed)
+    logs = [
+        jnp.where(j < accepted, summed - sums[j] + gate_ref[j], -jnp.inf) for j in range(length)
+    ]
+    top_log = summed + max_ref[...]
+    for log in logs:
+        top_log = jnp.maximum(top_log, log)
+    max_out[...] = top_log
+    weights = [jnp.exp(log - top_log) for log in logs]
+    keep = jnp.exp(summed + max_ref[...] - top_log)
+
+    krows[...] = jnp.zeros_like(krows)
+    vrows[...] = jnp.zeros_like(vrows)
+    scaled[...] = jnp.zeros_like(scaled)
+    for n in range(seqs):
+        krows[n * length : (n + 1) * length] = keys_ref[n].astype(jnp.float32)
+        vrows[n * length : (n + 1) * length] = values_ref[n].astype(jnp.float32)
+    values = vrows[...].astype(jnp.bfloat16)
+    values = jnp.concatenate([values, values], axis=0)
+    lane_seq = lax.broadcasted_iota(jnp.int32, (key_width, 2 * stride), 1) % stride // length
+    pick_seq = (
+        lax.broadcasted_iota(jnp.int32, (seqs, 2 * stride), 1) % stride // length
+        == lax.broadcasted_iota(jnp.int32, (seqs, 2 * stride), 0)
+    ).astype(jnp.bfloat16)
+
+    def fold(h):
+        column = jnp.zeros((rows, seqs), jnp.float32)
+        for j in range(length):
+            column = column + jnp.where(belongs & (row_pos == j), weights[j][h : h + 1], 0.0)
+        column = jnp.sum(column, axis=1, keepdims=True)
+        keys = krows[:rows, h * key_width : (h + 1) * key_width] * key_scale * column
+        high = keys.astype(jnp.bfloat16).astype(jnp.float32)
+        scaled[h, :rows] = high
+        scaled[h, stride : stride + rows] = keys - high
+        block_keys = scaled[h]
+        upright = block_keys.T
+        mine = values[:, h * value_width : (h + 1) * value_width]
+        for n in range(seqs):
+            left = jnp.where(lane_seq == n, upright, 0.0).astype(jnp.bfloat16)
+            update = jnp.dot(left, mine, preferred_element_type=jnp.float32)
+            fresh = keep[h : h + 1, n : n + 1] * mem_out[n, h] + update
+            mem_out[n, h] = fresh
+            mem16[h, n * key_width : (n + 1) * key_width] = fresh.astype(jnp.bfloat16)
+        carry = jnp.sum(jnp.where(diagonal, keep[h : h + 1], 0.0), axis=1, keepdims=True)
+        added = jnp.dot(pick_seq, block_keys.astype(jnp.bfloat16), preferred_element_type=jnp.float32)
+        norm_out[:, h, :] = carry * norm_ref[:, h, :] + added
+
     for t in t_peers:
         remote(tok_ref, xfull.at[t], tok_send.at[0], tok_recv.at[t], {"tp": t}).wait_recv()
 
@@ -300,10 +268,6 @@
     col_id = lax.broadcasted_iota(jnp.int32, (rows, rows), 1)
     causal = (row_id // length == col_id // length) & (col_id <= row_id)
     same = row_id == col_id
-    belongs = (
-        lax.broadcasted_iota(jnp.int32, (rows, seqs), 0) // length
-        == lax.broadcasted_iota(jnp.int32, (rows, seqs), 1)
-    )
     head_id = lax.broadcasted_iota(jnp.int32, gate_i.shape, 1)
 
     def turned(column):
@@ -316,7 +280,7 @@
         log_forget = jnp.sum(jnp.where(chosen, gate_f, 0.0), axis=1, keepdims=True)
         running = jnp.sum(jnp.where(causal, turned(log_forget), 0.0), axis=1, keepdims=True)
         within = jnp.where(causal, running + turned(in_gate - running), -jnp.inf)
-        base_max = jnp.sum(jnp.where(belongs, max_ref[h : h + 1], 0.0), axis=1, keepdims=True)
+        base_max = jnp.sum(jnp.where(belongs, top_log[h : h + 1], 0.0), axis=1, keepdims=True)
         top = jnp.maximum(running + base_max, jnp.max(within, axis=1, keepdims=True))
         decays.append(jnp.exp(within - top) * key_scale)
         carries.append(jnp.exp(running + base_max - top))
@@ -405,7 +369,7 @@
                 held = jnp.dot(spread, mem16[h], preferred_element_type=jnp.float32)
                 carried[h] = held * carries[h]
                 against = lax.dot_general(
-                    query, norm_ref[:, h, :], dims, precision=highest,
+                    query, norm_out[:, h, :], dims, precision=highest,
                     preferred_element_type=jnp.float32,
                 )
                 kept["norm", h] = carries[h] * jnp.sum(
@@ -440,11 +404,11 @@
 
     for c in range(chunks + 2):
         if c < chunks:
-            relay(c)
             if c == 0:
                 mem_copy.wait()
+            relay(c)
             for h in range(c, heads, 2) if c < 2 else ():
-                mem16[h] = memv[:, h].reshape(seqs * key_width, value_width).astype(jnp.bfloat16)
+                fold(h)
         if 1 <= c <= chunks:
             partial(c - 1)
         if c >= 2:
@@ -453,7 +417,24 @@
         copy.wait_send()
 
 
-def project(
+def write_kernel(*refs):
+    count = (len(refs) - 1) // 2
+    sems = refs[-1]
+    copies = []
+    for src, dst in zip(refs[:count], refs[count : 2 * count]):
+        if len(src.shape) == 4:
+            for n in range(src.shape[0]):
+                copies.append((src.at[n], dst.at[n]))
+        else:
+            copies.append((src, dst))
+    copies = [pltpu.make_async_copy(s, d, sems.at[i]) for i, (s, d) in enumerate(copies)]
+    for copy in copies:
+        copy.start()
+    for copy in copies:
+        copy.wait()
+
+
+def step(
     tokens,
     norm_gain,
     w_query,
@@ -463,15 +444,20 @@
     w_fgate,
     igate_bias,
     fgate_bias,
-    base_mem,
-    base_norm,
-    base_max,
+    prev_keys,
+    prev_values,
+    prev_igate,
+    prev_logf,
+    accepted,
+    state_mem,
+    state_norm,
+    state_max,
     kv_n,
     tp_n,
 ):
     seqs, length, part = tokens.shape
     rows = seqs * length
-    heads, key_width, value_width = base_mem.shape[1:]
+    heads, key_width, value_width = state_mem.shape[1:]
     depth, width = w_query.shape
     chunks = 2 + w_value.shape[1] // width
     reduce_n, group_n = factor(kv_n)
@@ -481,15 +467,39 @@
     dma = pltpu.SemaphoreType.DMA
     peers = max(1, outer_n + inner_n - 2)
     vmem = pl.BlockSpec(memory_space=pltpu.VMEM)
-    return pl.pallas_call(
-        functools.partial(project_kernel, reduce_n, outer_n, inner_n, tp_n),
-        out_shape=jax.ShapeDtypeStruct((seqs, length, heads * value_width), jnp.bfloat16),
-        in_specs=[vmem] * 9 + [pl.BlockSpec(memory_space=pl.ANY), vmem, vmem],
-        out_specs=vmem,
-        scratch_shapes=[
+    hbm = pl.BlockSpec(memory_space=pl.ANY)
+    small = (
+        norm_gain.reshape(1, -1),
+        w_igate.T,
+        w_fgate.T,
+        igate_bias.reshape(1, -1),
+        fgate_bias.reshape(1, -1),
+        prev_keys,
+        prev_values,
+        prev_igate.transpose(1, 2, 0),
+        prev_logf.transpose(1, 2, 0),
+        accepted.reshape(1, -1),
+        state_norm,
+        state_max.T,
+    )
+    results = (
+        jax.ShapeDtypeStruct((seqs, length, heads * value_width), jnp.bfloat16),
+        jax.ShapeDtypeStruct(state_mem.shape, jnp.float32),
+        jax.ShapeDtypeStruct(state_norm.shape, jnp.float32),
+        jax.ShapeDtypeStruct((heads, seqs), jnp.float32),
+    )
+    held = pl.pallas_call(
+        functools.partial(step_kernel, reduce_n, outer_n, inner_n, tp_n),
+        out_shape=results,
+        in_specs=[hbm] * (5 + len(small)),
+        out_specs=[vmem] * len(results),
+        scratch_shapes=[pltpu.VMEM(x.shape, x.dtype) for x in small]
+        + [
             pltpu.VMEM((tp_n, seqs, length, part), jnp.bfloat16),
             pltpu.VMEM((tp_n, rows, part), jnp.float32),
-            pltpu.VMEM(base_mem.shape, jnp.float32),
+            pltpu.VMEM((stride, heads * key_width), jnp.float32),
+            pltpu.VMEM((stride, heads * value_width), jnp.float32),
+            pltpu.VMEM((heads, 2 * stride, key_width), jnp.float32),
             pltpu.VMEM((heads, seqs * key_width, value_width), jnp.bfloat16),
             pltpu.VMEM((heads, rows, value_width), jnp.float32),
             pltpu.VMEM((reduce_n, rows, block), jnp.bfloat16),
@@ -515,65 +525,26 @@
             dma((chunks, reduce_n)),
             dma((chunks, reduce_n)),
             dma,
+            dma((len(small),)),
         ],
-        compiler_params=pltpu.CompilerParams(collective_id=0, has_side_effects=True),
-        name="project",
-    )(
-        tokens,
-        norm_gain.reshape(1, -1),
-        w_query,
-        w_key,
-        w_value,
-        w_igate.T,
-        w_fgate.T,
-        igate_bias.reshape(1, -1),
-        fgate_bias.reshape(1, -1),
-        base_mem,
-        base_norm,
-        base_max,
-    )
-
-
-def shards(
-    kv_n,
-    tp_n,
-    tokens,
-    norm_gain,
-    w_query,
-    w_key,
-    w_value,
-    w_igate,
-    w_fgate,
-    igate_bias,
-    fgate_bias,
-    prev_keys,
-    prev_values,
-    prev_igate,
-    prev_logf,
-    accepted,
-    state_mem,
-    state_norm,
-    state_max,
-):
-    base_mem, base_norm, base_max = fold_accepted(
-        prev_keys, prev_values, prev_igate, prev_logf, accepted, state_mem, state_norm, state_max
-    )
-    readout = project(
-        tokens,
-        norm_gain,
-        w_query,
-        w_key,
-        w_value,
-        w_igate,
-        w_fgate,
-        igate_bias,
-        fgate_bias,
-        base_mem,
-        base_norm,
-        base_max,
-        kv_n,
-        tp_n,
-    )
+        compiler_params=pltpu.CompilerParams(
+            collective_id=0, has_side_effects=True, vmem_limit_bytes=40 * 2**20
+        ),
+        name="step",
+    )(*(pltpu.with_memory_space_constraint(x, pltpu.HBM) for x in (tokens, w_query, w_key, w_value, state_mem) + small))
+    return pl.pallas_call(
+        write_kernel,
+        out_shape=results,
+        in_specs=[vmem] * len(results),
+        out_specs=[hbm] * len(results),
+        scratch_shapes=[dma((seqs + len(results),))],
+        compiler_params=pltpu.CompilerParams(vmem_limit_bytes=8 * 2**20),
+        name="write",
+    )(*held)
+
+
+def shards(kv_n, tp_n, *args):
+    readout, base_mem, base_norm, base_max = step(*args, kv_n, tp_n)
     return (readout, base_mem, base_norm, base_max.T)
 
 

time: 45.5 us -> 35.1 us (0.77)
  Pallas kernels: 42.9 us -> 34.3 us
  local copies, waits for them, and re-layouts: 1.55 us -> 0 us
    pallas_call x2, Pallas kernels: 42.9 us -> 34.3 us  [the longest x1 31.8 us: step(): pl.pallas_call(functools.partial(step_kernel, reduce_n, outer_n, inner_n,...]
    unnamed x1 -> x0, local copies, waits for them, and re-layouts: 1.55 us -> none
where the time goes in v1:
time: 35.1 us; the launch traced here: 34.9 us
  Pallas kernels  34.3 us (98%)
  between operations  0.65 us (2%)
    pallas_call x1, Pallas kernels, step(): pl.pallas_call(functools.partial(step_kernel, reduce_n, outer_n, inner_n,...  31.8 us
    pallas_call x1, Pallas kernels, step(): pl.pallas_call(write_kernel, out_shape=results, in_specs=[vmem] * len(res...  2.49 us

profile of v1, /device:TPU:0, one launch (start us, length us, event | category | flops | bytes accessed | tf_op | source)
XLA Modules:
  0.0 34.9 jit_solution(13229678117197483774)
XLA Ops:
  0.6 31.8 %step.1 = (bf16[10,3,1024]{2,1,0:T(4,128)(2,1)S(1)}, f32[10,4,128,256]{3,2,1,0:T(8,128)S(1)}, f32[10,4,128]{2,1,0:T(4,128)S(1)}, f32[4,10]{1,0:T(4,128)S(1)}) custom-call(bf16[10,3,1024]{2,1,0:T(4,128)(2,1)} %tok_ref.1, bf16[128,512]{1,0:T(8,128)(2,1)} %wq_ref.1, bf16[128,512]{1,0:T(8,128)(2,1)} %wk_ref.1, bf16[128,1024]{1,0:T(8,128)(2,1)} %wv_ref.1, ...), custom_call_target="tpu_custom_call" | custom-call | tf_op jit(solution)/shard_map/step/pallas_call | solution.py:491
  32.4 2.5 %write.1 = (bf16[10,3,1024]{2,1,0:T(4,128)(2,1)}, f32[10,4,128,256]{3,2,1,0:T(8,128)}, f32[10,4,128]{2,1,0:T(4,128)}, f32[4,10]{1,0:T(4,128)}) custom-call(bf16[10,3,1024]{2,1,0:T(4,128)(2,1)S(1)} %get-tuple-element.12.refs_0_, f32[10,4,128,256]{3,2,1,0:T(8,128)S(1)} %get-tuple-element.13.refs_1_, f32[10,4,128]{2,1,0:T(4,128)S(1)} %get-tuple-element.14.refs_2_, ...), custom_call_target="tpu_custom_call" | custom-call | tf_op jit(solution)/shard_map/write/pallas_call | solution.py:535

commit v2 on v1

--- a/solution.py
+++ b/solution.py
@@ -8,6 +8,7 @@
 from jax.sharding import PartitionSpec as P
 
 epsilon = 1e-06
+pool = 12
 highest = lax.Precision.HIGHEST
 
 
@@ -60,26 +61,21 @@
         abuf,
         xall,
         wbuf,
-        pbuf,
         own,
         sbuf,
         rbuf,
         tok_local,
-        tok_send,
+        send_sem,
         tok_recv,
-        a_send,
         a_recv,
         w_local,
-        w_send,
         w_recv,
-        fy_send,
-        fx_send,
-        fy_recv,
-        fx_recv,
-        p_send,
+        f_recv,
         p_recv,
         mem_sem,
         small_sem,
+        up_sem,
+        down_sem,
     ) = refs
     group_n = outer_n * inner_n
     chunks, rows_all, width = wbuf.shape
@@ -103,17 +99,31 @@
 
     x_peers = [outer * inner_n + (inner + d) % inner_n for d in range(1, inner_n)]
     y_peers = [((outer + d) % outer_n) * inner_n + inner for d in range(1, outer_n)]
+    t_peers = [(tp + d) % tp_n for d in range(1, tp_n)]
+    x_back = [outer * inner_n + (inner + inner_n - d) % inner_n for d in range(1, inner_n)]
+    y_back = [((outer + outer_n - d) % outer_n) * inner_n + inner for d in range(1, outer_n)]
     r_peers = [(red + d) % reduce_n for d in range(1, reduce_n)]
-    t_peers = [(tp + d) % tp_n for d in range(1, tp_n)]
+    r_back = [(red + reduce_n - d) % reduce_n for d in range(1, reduce_n)]
+    t_back = [(tp + tp_n - d) % tp_n for d in range(1, tp_n)]
 
     barrier = pltpu.get_barrier_semaphore()
     targets = (
         [{"tp": t} for t in t_peers]
         + [at_grp(p) for p in x_peers + y_peers]
-        + [{"kv": p * group_n + grp} for p in r_peers]
     )
+
+    def signal(sem, target):
+        pl.semaphore_signal(sem, inc=1, device_id=target, device_id_type=pl.DeviceIdType.MESH)
+
+    def at_red(index):
+        return {"kv": index * group_n + grp}
+
     for target in targets:
-        pl.semaphore_signal(barrier, inc=1, device_id=target, device_id_type=pl.DeviceIdType.MESH)
+        signal(barrier, target)
+    has_below, has_above = red > 0, red < reduce_n - 1
+    if reduce_n > 1:
+        pl.when(has_below)(lambda: signal(barrier, at_red(red - 1)))
+        pl.when(has_above)(lambda: signal(barrier, at_red(red + 1)))
 
     def chunk_of(c):
         if c == 0:
@@ -152,26 +162,63 @@
     mem_copy.start()
     for copy in locals_:
         copy.wait()
-    pl.semaphore_wait(barrier, len(targets))
+    greeted = len(targets)
+    if reduce_n > 1:
+        greeted = greeted + jnp.minimum(red, 1) + jnp.minimum(reduce_n - 1 - red, 1)
+    pl.semaphore_wait(barrier, greeted)
 
     sends = []
 
-    def go(copy):
+    def go(src, dst, recv, target):
+        count = len(sends)
+        if count >= pool:
+            sends[count - pool].wait_send()
+        copy = remote(src, dst, send_sem.at[count % pool], recv, target)
         copy.start()
         sends.append(copy)
 
     for i, t in enumerate(t_peers):
-        go(remote(xfull.at[tp], xfull.at[tp], tok_send.at[i], tok_recv.at[tp], {"tp": t}))
+        go(xfull.at[tp], xfull.at[tp], tok_recv.at[i], {"tp": t})
 
     def direct(c):
         for i, p in enumerate(x_peers + y_peers):
-            go(remote(slot(c, grp), slot(c, grp), w_send.at[c, i], w_recv.at[c, grp], at_grp(p)))
+            go(slot(c, grp), slot(c, grp), w_recv.at[c, i], at_grp(p))
 
     direct(0)
     if chunks > 1:
         direct(1)
 
-    for copy in small:
+    if reduce_n > 2:
+        last = reduce_n - 1
+        pl.when(red == 1)(lambda: signal(up_sem, at_red(red + 1)))
+        pl.when(red == last - 1)(lambda: signal(down_sem, at_red(red - 1)))
+        pl.when(red >= 2)(lambda: pl.semaphore_wait(up_sem, 1))
+        pl.when((red >= 2) & (red < last))(lambda: signal(up_sem, at_red(red + 1)))
+        pl.when(red <= last - 2)(lambda: pl.semaphore_wait(down_sem, 1))
+        pl.when((red <= last - 2) & (red > 0))(lambda: signal(down_sem, at_red(red - 1)))
+
+    for i, t in enumerate(t_back):
+        remote(xfull.at[t], xfull.at[t], send_sem.at[0], tok_recv.at[i], {"tp": t}).wait_recv()
+
+    small[0].wait()
+    total = jnp.zeros((rows, 1), jnp.float32)
+    for t in range(tp_n):
+        for n in range(seqs):
+            xrows[t, n * length : (n + 1) * length] = xfull[t, n].astype(jnp.float32)
+        piece = xrows[t]
+        total = total + jnp.sum(piece * piece, axis=1, keepdims=True)
+    factor_rows = lax.rsqrt(total / (tp_n * part) + epsilon)
+    step = min(block, part)
+    for p in range(reduce_n * block // step):
+        first = p * step
+        piece = xrows[first // part, :, first % part : first % part + step]
+        normed = (piece * factor_rows * gain_ref[:, first : first + step]).astype(jnp.bfloat16)
+        nbuf[first // block, :, first % block : first % block + step] = normed
+
+    for i, p in enumerate(r_peers):
+        go(nbuf.at[p], abuf.at[i], a_recv, {"kv": p * group_n + grp})
+
+    for copy in small[1:]:
         copy.wait()
 
     row_seq = lax.broadcasted_iota(jnp.int32, (rows, seqs), 0) // length
@@ -233,27 +280,6 @@
         added = jnp.dot(pick_seq, block_keys.astype(jnp.bfloat16), preferred_element_type=jnp.float32)
         norm_out[:, h, :] = carry * norm_ref[:, h, :] + added
 
-    for t in t_peers:
-        remote(tok_ref, xfull.at[t], tok_send.at[0], tok_recv.at[t], {"tp": t}).wait_recv()
-
-    total = jnp.zeros((rows, 1), jnp.float32)
-    for t in range(tp_n):
-        for n in range(seqs):
-            xrows[t, n * length : (n + 1) * length] = xfull[t, n].astype(jnp.float32)
-        piece = xrows[t]
-        total = total + jnp.sum(piece * piece, axis=1, keepdims=True)
-    factor_rows = lax.rsqrt(total / (tp_n * part) + epsilon)
-    step = min(block, part)
-    for p in range(reduce_n * block // step):
-        first = p * step
-        piece = xrows[first // part, :, first % part : first % part + step]
-        normed = (piece * factor_rows * gain_ref[:, first : first + step]).astype(jnp.bfloat16)
-        nbuf[first // block, :, first % block : first % block + step] = normed
-
-    for i, p in enumerate(r_peers):
-        go(remote(nbuf.at[p], abuf.at[red], a_send.at[i], a_recv.at[red], {"kv": p * group_n + grp}))
-    abuf[red] = nbuf[red]
-
     dims = (((1,), (1,)), ((), ()))
     gate_i = jnp.zeros((rows, wi_ref.shape[0]), jnp.float32)
     gate_f = jnp.zeros((rows, wf_ref.shape[0]), jnp.float32)
@@ -286,71 +312,50 @@
         carries.append(jnp.exp(running + base_max - top))
         tops.append(jnp.exp(-top))
 
-    xall[...] = jnp.zeros_like(xall)
-    for p in r_peers:
-        remote(nbuf.at[p], abuf.at[p], a_send.at[0], a_recv.at[p], {"kv": p * group_n + grp}).wait_recv()
-    for p in range(reduce_n):
-        xall[p * stride : p * stride + rows, :] = abuf[p]
+    def receive_rows():
+        xall[...] = jnp.zeros_like(xall)
+        xall[:rows, :] = nbuf[red]
+        if reduce_n > 1:
+            remote(abuf, abuf, send_sem.at[0], a_recv, {"kv": r_back[0] * group_n + grp}).wait_recv()
+        for i in range(reduce_n - 1):
+            xall[(i + 1) * stride : (i + 1) * stride + rows, :] = abuf[i]
 
     def relay(c):
-        for i, p in enumerate(x_peers):
-            remote(chunk_of(c), slot(c, p), w_send.at[c, 0], w_recv.at[c, p], at_grp(p)).wait_recv()
+        for i, p in enumerate(x_back):
+            remote(slot(c, p), slot(c, p), send_sem.at[0], w_recv.at[c, i], at_grp(p)).wait_recv()
             for j, q in enumerate(y_peers):
-                go(
-                    remote(
-                        slot(c, p, 0, half),
-                        slot(c, p, 0, half),
-                        fy_send.at[c, i, j],
-                        fy_recv.at[c, p],
-                        at_grp(q),
-                    )
-                )
-        for j, q in enumerate(y_peers):
-            remote(chunk_of(c), slot(c, q), w_send.at[c, 0], w_recv.at[c, q], at_grp(q)).wait_recv()
+                piece = slot(c, p, 0, half)
+                go(piece, piece, f_recv.at[c, i, j], at_grp(q))
+        for j, q in enumerate(y_back):
+            k = len(x_back) + j
+            remote(slot(c, q), slot(c, q), send_sem.at[0], w_recv.at[c, k], at_grp(q)).wait_recv()
             for i, p in enumerate(x_peers):
-                go(
-                    remote(
-                        slot(c, q, half, half),
-                        slot(c, q, half, half),
-                        fx_send.at[c, i, j],
-                        fx_recv.at[c, q],
-                        at_grp(p),
-                    )
-                )
+                piece = slot(c, q, half, half)
+                go(piece, piece, f_recv.at[c, i, j], at_grp(p))
         if c + 2 < chunks:
             direct(c + 2)
 
     def partial(c):
-        for i in range(1, inner_n):
-            for j in range(1, outer_n):
-                source = ((outer + j) % outer_n) * inner_n + (inner + i) % inner_n
-                for start, send, recv in ((0, fy_send, fy_recv), (half, fx_send, fx_recv)):
-                    here = slot(c, source, start, half)
-                    remote(here, here, send.at[c, 0, 0], recv.at[c, source], at_grp(source)).wait_recv()
+        for i, p in enumerate(x_back):
+            for j, q in enumerate(y_back):
+                source = q - inner + p - outer * inner_n
+                here = slot(c, source)
+                remote(here, here, send_sem.at[0], f_recv.at[c, i, j], at_grp(source)).wait_recv()
         product = jnp.dot(xall[...], wbuf[c], preferred_element_type=jnp.float32)
-        for p in range(reduce_n):
-            piece = product[p * stride : p * stride + rows]
-            pbuf[p] = piece
-            sbuf[c, p] = piece.astype(jnp.bfloat16)
-        own[c] = pbuf[red]
-        for i, p in enumerate(r_peers):
-            go(
-                remote(
-                    sbuf.at[c, p],
-                    rbuf.at[c, red],
-                    p_send.at[c, i],
-                    p_recv.at[c, red],
-                    {"kv": p * group_n + grp},
-                )
-            )
+        own[c] = product[:rows]
+        for i, p in reversed(list(enumerate(r_back))):
+            piece = product[(i + 1) * stride : (i + 1) * stride + rows]
+            sbuf[c, i] = piece.astype(jnp.bfloat16)
+            go(sbuf.at[c, i], rbuf.at[c, i], p_recv.at[c], {"kv": p * group_n + grp})
 
     def settle(c):
         total = own[c]
-        for p in r_peers:
-            remote(
-                sbuf.at[c, p], rbuf.at[c, p], p_send.at[c, 0], p_recv.at[c, p], {"kv": p * group_n + grp}
-            ).wait_recv()
-            total = total + rbuf[c, p].astype(jnp.float32)
+        if reduce_n > 1:
+            here = rbuf.at[c]
+            source = {"kv": r_back[0] * group_n + grp}
+            remote(here, here, send_sem.at[0], p_recv.at[c], source).wait_recv()
+        for i in range(reduce_n - 1):
+            total = total + rbuf[c, i].astype(jnp.float32)
         return total.astype(jnp.bfloat16)
 
     kept = {}
@@ -402,18 +407,20 @@
                         n * length : (n + 1) * length
                     ].astype(jnp.bfloat16)
 
-    for c in range(chunks + 2):
+    for c in range(chunks + 3):
         if c < chunks:
             if c == 0:
                 mem_copy.wait()
             relay(c)
             for h in range(c, heads, 2) if c < 2 else ():
                 fold(h)
+        if c == 1:
+            receive_rows()
         if 1 <= c <= chunks:
             partial(c - 1)
-        if c >= 2:
-            finish(c - 2)
-    for copy in sends:
+        if c >= 3:
+            finish(c - 3)
+    for copy in sends[-pool:]:
         copy.wait_send()
 
 
@@ -422,11 +429,7 @@
     sems = refs[-1]
     copies = []
     for src, dst in zip(refs[:count], refs[count : 2 * count]):
-        if len(src.shape) == 4:
-            for n in range(src.shape[0]):
-                copies.append((src.at[n], dst.at[n]))
-        else:
-            copies.append((src, dst))
+        copies.append((src, dst))
     copies = [pltpu.make_async_copy(s, d, sems.at[i]) for i, (s, d) in enumerate(copies)]
     for copy in copies:
         copy.start()
@@ -466,6 +469,8 @@
     stride = -(-rows // 16) * 16
     dma = pltpu.SemaphoreType.DMA
     peers = max(1, outer_n + inner_n - 2)
+    others = max(1, reduce_n - 1)
+    relays = (max(1, inner_n - 1), max(1, outer_n - 1))
     vmem = pl.BlockSpec(memory_space=pltpu.VMEM)
     hbm = pl.BlockSpec(memory_space=pl.ANY)
     small = (
@@ -503,29 +508,24 @@
             pltpu.VMEM((heads, seqs * key_width, value_width), jnp.bfloat16),
             pltpu.VMEM((heads, rows, value_width), jnp.float32),
             pltpu.VMEM((reduce_n, rows, block), jnp.bfloat16),
-            pltpu.VMEM((reduce_n, rows, block), jnp.bfloat16),
+            pltpu.VMEM((others, rows, block), jnp.bfloat16),
             pltpu.VMEM((reduce_n * stride, block), jnp.bfloat16),
             pltpu.VMEM((chunks, block, width), jnp.bfloat16),
-            pltpu.VMEM((reduce_n, rows, width), jnp.float32),
             pltpu.VMEM((chunks, rows, width), jnp.float32),
-            pltpu.VMEM((chunks, reduce_n, rows, width), jnp.bfloat16),
-            pltpu.VMEM((chunks, reduce_n, rows, width), jnp.bfloat16),
+            pltpu.VMEM((chunks, others, rows, width), jnp.bfloat16),
+            pltpu.VMEM((chunks, others, rows, width), jnp.bfloat16),
             dma,
-            dma((tp_n,)),
-            dma((tp_n,)),
-            dma((reduce_n,)),
-            dma((reduce_n,)),
+            dma((pool,)),
+            dma((max(1, tp_n - 1),)),
+            dma,
             dma((chunks,)),
             dma((chunks, peers)),
-            dma((chunks, group_n)),
-            dma((chunks, inner_n, outer_n)),
-            dma((chunks, inner_n, outer_n)),
-            dma((chunks, group_n)),
-            dma((chunks, group_n)),
-            dma((chunks, reduce_n)),
-            dma((chunks, reduce_n)),
+            dma((chunks,) + relays),
+            dma((chunks,)),
             dma,
             dma((len(small),)),
+            pltpu.SemaphoreType.REGULAR,
+            pltpu.SemaphoreType.REGULAR,
         ],
         compiler_params=pltpu.CompilerParams(
             collective_id=0, has_side_effects=True, vmem_limit_bytes=40 * 2**20

time: 35.1 us -> 33.4 us (0.952)
  Pallas kernels: 34.3 us -> 32.6 us
    pallas_call x1, Pallas kernels: 31.8 us -> 30 us  [step(): pl.pallas_call(functools.partial(step_kernel, reduce_n, outer_n, inner_n,...]
where the time goes in v2:
time: 33.4 us; the launch traced here: 33.2 us
  Pallas kernels  32.6 us (98%)
  between operations  0.65 us (2%)
    pallas_call x1, Pallas kernels, step(): pl.pallas_call(functools.partial(step_kernel, reduce_n, outer_n, inner_n,...  30 us
    pallas_call x1, Pallas kernels, step(): pl.pallas_call(write_kernel, out_shape=results, in_specs=[vmem] * len(res...  2.52 us

profile of v2, /device:TPU:0, one launch (start us, length us, event | category | flops | bytes accessed | tf_op | source)
XLA Modules:
  0.0 33.2 jit_solution(15466185278804199388)
XLA Ops:
  0.6 30.0 %step.1 = (bf16[10,3,1024]{2,1,0:T(4,128)(2,1)S(1)}, f32[10,4,128,256]{3,2,1,0:T(8,128)S(1)}, f32[10,4,128]{2,1,0:T(4,128)S(1)}, f32[4,10]{1,0:T(4,128)S(1)}) custom-call(bf16[10,3,1024]{2,1,0:T(4,128)(2,1)} %tok_ref.1, bf16[128,512]{1,0:T(8,128)(2,1)} %wq_ref.1, bf16[128,512]{1,0:T(8,128)(2,1)} %wk_ref.1, bf16[128,1024]{1,0:T(8,128)(2,1)} %wv_ref.1, ...), custom_call_target="tpu_custom_call" | custom-call | tf_op jit(solution)/shard_map/step/pallas_call | solution.py:496
  30.7 2.5 %write.1 = (bf16[10,3,1024]{2,1,0:T(4,128)(2,1)}, f32[10,4,128,256]{3,2,1,0:T(8,128)}, f32[10,4,128]{2,1,0:T(4,128)}, f32[4,10]{1,0:T(4,128)}) custom-call(bf16[10,3,1024]{2,1,0:T(4,128)(2,1)S(1)} %get-tuple-element.12.refs_0_, f32[10,4,128,256]{3,2,1,0:T(8,128)S(1)} %get-tuple-element.13.refs_1_, f32[10,4,128]{2,1,0:T(4,128)S(1)} %get-tuple-element.14.refs_2_, ...), custom_call_target="tpu_custom_call" | custom-call | tf_op jit(solution)/shard_map/write/pallas_call | solution.py:535

commit v3 on v2

--- a/solution.py
+++ b/solution.py
@@ -1,4 +1,5 @@
 import functools
+import math
 
 import jax
 import jax.numpy as jnp
@@ -8,7 +9,7 @@
 from jax.sharding import PartitionSpec as P
 
 epsilon = 1e-06
-pool = 12
+pool = 10
 highest = lax.Precision.HIGHEST
 
 
@@ -24,6 +25,7 @@
     outer_n,
     inner_n,
     tp_n,
+    turned_chunk,
     tok_ref,
     wq_ref,
     wk_ref,
@@ -60,6 +62,9 @@
         nbuf,
         abuf,
         xall,
+        nturn,
+        aturn,
+        xturn,
         wbuf,
         own,
         sbuf,
@@ -76,11 +81,13 @@
         small_sem,
         up_sem,
         down_sem,
+        side_sem,
+        turn_recv,
     ) = refs
     group_n = outer_n * inner_n
     chunks, rows_all, width = wbuf.shape
     depth = rows_all // group_n
-    half = depth // 2
+    cut = depth * 5 // 128 * 16 if turned_chunk is not None else depth // 2
     seqs, length, part = tok_ref.shape
     rows = seqs * length
     heads, _, value_width = mem16.shape
@@ -106,6 +113,17 @@
     r_back = [(red + reduce_n - d) % reduce_n for d in range(1, reduce_n)]
     t_back = [(tp + tp_n - d) % tp_n for d in range(1, tp_n)]
 
+    high_n = max(1, reduce_n // 2)
+    high, low = red // 2, red % 2
+    low_kv = (high * 2 + 1 - low) * group_n + grp
+    steps = [(dh, dy) for dh in range(high_n) for dy in range(outer_n)][1:]
+    turned_back = [
+        ((high + high_n - dh) % high_n, (outer + outer_n - dy) % outer_n) for dh, dy in steps
+    ]
+
+    def turned_kv(h, y):
+        return {"kv": (h * 2 + low) * group_n + y * inner_n + inner}
+
     barrier = pltpu.get_barrier_semaphore()
     targets = (
         [{"tp": t} for t in t_peers]
@@ -134,8 +152,11 @@
 
     def slot(c, source, start=0, size=None):
         size = depth if size is None else size
-        first = pl.multiple_of(source * depth + start, half)
+        first = pl.multiple_of(source * depth + start, math.gcd(depth, start))
         return wbuf.at[c, pl.ds(first, size), :]
+
+    def home(c):
+        return low * inner_n + inner if c == turned_chunk else grp
 
     def remote(src, dst, send, recv, target):
         return pltpu.make_async_remote_copy(
@@ -147,10 +168,11 @@
             device_id_type=pl.DeviceIdType.MESH,
         )
 
-    locals_ = [pltpu.make_async_copy(tok_ref, xfull.at[tp], tok_local)]
-    for c in range(chunks):
-        locals_.append(pltpu.make_async_copy(chunk_of(c), slot(c, grp), w_local.at[c]))
-    for copy in locals_:
+    tok_copy = pltpu.make_async_copy(tok_ref, xfull.at[tp], tok_local)
+    w_copies = [
+        pltpu.make_async_copy(chunk_of(c), slot(c, home(c)), w_local.at[c]) for c in range(chunks)
+    ]
+    for copy in w_copies[:1] + [tok_copy] + w_copies[1:]:
         copy.start()
     small = [
         pltpu.make_async_copy(src, dst, small_sem.at[i])
@@ -160,8 +182,6 @@
         copy.start()
     mem_copy = pltpu.make_async_copy(mem_ref, mem_out, mem_sem)
     mem_copy.start()
-    for copy in locals_:
-        copy.wait()
     greeted = len(targets)
     if reduce_n > 1:
         greeted = greeted + jnp.minimum(red, 1) + jnp.minimum(reduce_n - 1 - red, 1)
@@ -177,14 +197,17 @@
         copy.start()
         sends.append(copy)
 
+    def direct(c):
+        w_copies[c].wait()
+        here = slot(c, home(c))
+        second = [{"kv": low_kv}] if c == turned_chunk else [at_grp(p) for p in y_peers]
+        for i, target in enumerate([at_grp(p) for p in x_peers] + second):
+            go(here, here, w_recv.at[c, i], target)
+
+    direct(0)
+    tok_copy.wait()
     for i, t in enumerate(t_peers):
         go(xfull.at[tp], xfull.at[tp], tok_recv.at[i], {"tp": t})
-
-    def direct(c):
-        for i, p in enumerate(x_peers + y_peers):
-            go(slot(c, grp), slot(c, grp), w_recv.at[c, i], at_grp(p))
-
-    direct(0)
     if chunks > 1:
         direct(1)
 
@@ -209,14 +232,30 @@
         total = total + jnp.sum(piece * piece, axis=1, keepdims=True)
     factor_rows = lax.rsqrt(total / (tp_n * part) + epsilon)
     step = min(block, part)
+    turned_spots = [
+        (h, y, a) for h in range(high_n) for y in range(outer_n) for a in range(2)
+    ] if turned_chunk is not None else []
     for p in range(reduce_n * block // step):
         first = p * step
         piece = xrows[first // part, :, first % part : first % part + step]
         normed = (piece * factor_rows * gain_ref[:, first : first + step]).astype(jnp.bfloat16)
         nbuf[first // block, :, first % block : first % block + step] = normed
+        for h, y, a in turned_spots:
+            begin = ((h * 2 + a) * group_n + y * inner_n) * depth - first
+            if 0 <= begin < step:
+                run = inner_n * depth
+                nturn[h * outer_n + y, :, a * run : (a + 1) * run] = normed[:, begin : begin + run]
 
     for i, p in enumerate(r_peers):
         go(nbuf.at[p], abuf.at[i], a_recv, {"kv": p * group_n + grp})
+    if turned_chunk is not None:
+        for dh in range(1, high_n):
+            signal(side_sem, turned_kv((high + dh) % high_n, outer))
+        if high_n > 1:
+            pl.semaphore_wait(side_sem, high_n - 1)
+        for i, (dh, dy) in enumerate(steps):
+            h, y = (high + dh) % high_n, (outer + dy) % outer_n
+            go(nturn.at[h * outer_n + y], aturn.at[i], turn_recv, turned_kv(h, y))
 
     for copy in small[1:]:
         copy.wait()
@@ -320,33 +359,64 @@
         for i in range(reduce_n - 1):
             xall[(i + 1) * stride : (i + 1) * stride + rows, :] = abuf[i]
 
+    def relay_turned(c):
+        for i, p in enumerate(x_back):
+            here = slot(c, low * inner_n + p % inner_n)
+            remote(here, here, send_sem.at[0], w_recv.at[c, i], at_grp(p)).wait_recv()
+            go(here, here, f_recv.at[c, i, 0], {"kv": low_kv})
+        k = len(x_back)
+        here = slot(c, (1 - low) * inner_n + inner)
+        remote(here, here, send_sem.at[0], w_recv.at[c, k], {"kv": low_kv}).wait_recv()
+        if c + 2 < chunks:
+            direct(c + 2)
+
     def relay(c):
+        if c == turned_chunk:
+            relay_turned(c)
+            return
         for i, p in enumerate(x_back):
             remote(slot(c, p), slot(c, p), send_sem.at[0], w_recv.at[c, i], at_grp(p)).wait_recv()
             for j, q in enumerate(y_peers):
-                piece = slot(c, p, 0, half)
+                piece = slot(c, p, 0, cut)
                 go(piece, piece, f_recv.at[c, i, j], at_grp(q))
         for j, q in enumerate(y_back):
             k = len(x_back) + j
             remote(slot(c, q), slot(c, q), send_sem.at[0], w_recv.at[c, k], at_grp(q)).wait_recv()
             for i, p in enumerate(x_peers):
-                piece = slot(c, q, half, half)
+                piece = slot(c, q, cut, depth - cut)
                 go(piece, piece, f_recv.at[c, i, j], at_grp(p))
         if c + 2 < chunks:
             direct(c + 2)
 
-    def partial(c):
+    def receive_turned():
+        xturn[...] = jnp.zeros_like(xturn)
+        xturn[:rows, :] = nturn[high * outer_n + outer]
+        remote(aturn, aturn, send_sem.at[0], turn_recv, turned_kv(*turned_back[0])).wait_recv()
+        for i in range(reduce_n - 1):
+            xturn[(i + 1) * stride : (i + 1) * stride + rows, :] = aturn[i]
+
+    def land(c):
         for i, p in enumerate(x_back):
             for j, q in enumerate(y_back):
                 source = q - inner + p - outer * inner_n
                 here = slot(c, source)
                 remote(here, here, send_sem.at[0], f_recv.at[c, i, j], at_grp(source)).wait_recv()
-        product = jnp.dot(xall[...], wbuf[c], preferred_element_type=jnp.float32)
+
+    def partial(c):
+        rows_in, owners = xall, [at_red(p) for p in r_back]
+        if c == turned_chunk:
+            rows_in, owners = xturn, [turned_kv(h, y) for h, y in turned_back]
+            for i, p in enumerate(x_back):
+                here = slot(c, (1 - low) * inner_n + p % inner_n)
+                remote(here, here, send_sem.at[0], f_recv.at[c, i, 0], {"kv": low_kv}).wait_recv()
+        else:
+            land(c)
+        product = jnp.dot(rows_in[...], wbuf[c], preferred_element_type=jnp.float32)
         own[c] = product[:rows]
-        for i, p in reversed(list(enumerate(r_back))):
+        for i, owner in reversed(list(enumerate(owners))):
             piece = product[(i + 1) * stride : (i + 1) * stride + rows]
             sbuf[c, i] = piece.astype(jnp.bfloat16)
-            go(sbuf.at[c, i], rbuf.at[c, i], p_recv.at[c], {"kv": p * group_n + grp})
+            go(sbuf.at[c, i], rbuf.at[c, i], p_recv.at[c], owner)
 
     def settle(c):
         total = own[c]
@@ -416,6 +486,8 @@
                 fold(h)
         if c == 1:
             receive_rows()
+            if turned_chunk is not None:
+                receive_turned()
         if 1 <= c <= chunks:
             partial(c - 1)
         if c >= 3:
@@ -469,6 +541,8 @@
     stride = -(-rows // 16) * 16
     dma = pltpu.SemaphoreType.DMA
     peers = max(1, outer_n + inner_n - 2)
+    square = outer_n == 2 and inner_n == 2 and reduce_n == 4 and (depth * inner_n) % 128 == 0
+    turned_chunk = 2 if square else None
     others = max(1, reduce_n - 1)
     relays = (max(1, inner_n - 1), max(1, outer_n - 1))
     vmem = pl.BlockSpec(memory_space=pltpu.VMEM)
@@ -494,7 +568,7 @@
         jax.ShapeDtypeStruct((heads, seqs), jnp.float32),
     )
     held = pl.pallas_call(
-        functools.partial(step_kernel, reduce_n, outer_n, inner_n, tp_n),
+        functools.partial(step_kernel, reduce_n, outer_n, inner_n, tp_n, turned_chunk),
         out_shape=results,
         in_specs=[hbm] * (5 + len(small)),
         out_specs=[vmem] * len(results),
@@ -507,6 +581,9 @@
             pltpu.VMEM((heads, 2 * stride, key_width), jnp.float32),
             pltpu.VMEM((heads, seqs * key_width, value_width), jnp.bfloat16),
             pltpu.VMEM((heads, rows, value_width), jnp.float32),
+            pltpu.VMEM((reduce_n, rows, block), jnp.bfloat16),
+            pltpu.VMEM((others, rows, block), jnp.bfloat16),
+            pltpu.VMEM((reduce_n * stride, block), jnp.bfloat16),
             pltpu.VMEM((reduce_n, rows, block), jnp.bfloat16),
             pltpu.VMEM((others, rows, block), jnp.bfloat16),
             pltpu.VMEM((reduce_n * stride, block), jnp.bfloat16),
@@ -526,6 +603,8 @@
             dma((len(small),)),
             pltpu.SemaphoreType.REGULAR,
             pltpu.SemaphoreType.REGULAR,
+            pltpu.SemaphoreType.REGULAR,
+            dma,
         ],
         compiler_params=pltpu.CompilerParams(
             collective_id=0, has_side_effects=True, vmem_limit_bytes=40 * 2**20

time: 33.4 us -> 32.6 us (0.976)
  Pallas kernels: 32.6 us -> 31.8 us
    pallas_call x1, Pallas kernels: 30 us -> 29.3 us  [step(): pl.pallas_call(functools.partial(step_kernel, reduce_n, outer_n, inner_n,...]
where the time goes in v3:
time: 32.6 us; the launch traced here: 32.5 us
  Pallas kernels  31.8 us (98%)
  between operations  0.65 us (2%)
    pallas_call x1, Pallas kernels, step(): pl.pallas_call(functools.partial(step_kernel, reduce_n, outer_n, inner_n,...  29.3 us
    pallas_call x1, Pallas kernels, step(): pl.pallas_call(write_kernel, out_shape=results, in_specs=[vmem] * len(res...  2.52 us

profile of v3, /device:TPU:0, one launch (start us, length us, event | category | flops | bytes accessed | tf_op | source)
XLA Modules:
  0.0 32.5 jit_solution(4738896267316606737)
XLA Ops:
  0.6 29.3 %step.1 = (bf16[10,3,1024]{2,1,0:T(4,128)(2,1)S(1)}, f32[10,4,128,256]{3,2,1,0:T(8,128)S(1)}, f32[10,4,128]{2,1,0:T(4,128)S(1)}, f32[4,10]{1,0:T(4,128)S(1)}) custom-call(bf16[10,3,1024]{2,1,0:T(4,128)(2,1)} %tok_ref.1, bf16[128,512]{1,0:T(8,128)(2,1)} %wq_ref.1, bf16[128,512]{1,0:T(8,128)(2,1)} %wk_ref.1, bf16[128,1024]{1,0:T(8,128)(2,1)} %wv_ref.1, ...), custom_call_target="tpu_custom_call" | custom-call | tf_op jit(solution)/shard_map/step/pallas_call | solution.py:570
  30.0 2.5 %write.1 = (bf16[10,3,1024]{2,1,0:T(4,128)(2,1)}, f32[10,4,128,256]{3,2,1,0:T(8,128)}, f32[10,4,128]{2,1,0:T(4,128)}, f32[4,10]{1,0:T(4,128)}) custom-call(bf16[10,3,1024]{2,1,0:T(4,128)(2,1)S(1)} %get-tuple-element.12.refs_0_, f32[10,4,128,256]{3,2,1,0:T(8,128)S(1)} %get-tuple-element.13.refs_1_, f32[10,4,128]{2,1,0:T(4,128)S(1)} %get-tuple-element.14.refs_2_, ...), custom_call_target="tpu_custom_call" | custom-call | tf_op jit(solution)/shard_map/write/pallas_call | solution.py:614

commit v4 on v3

--- a/solution.py
+++ b/solution.py
@@ -9,7 +9,7 @@
 from jax.sharding import PartitionSpec as P
 
 epsilon = 1e-06
-pool = 10
+pool = 6
 highest = lax.Precision.HIGHEST
 
 
@@ -248,14 +248,6 @@
 
     for i, p in enumerate(r_peers):
         go(nbuf.at[p], abuf.at[i], a_recv, {"kv": p * group_n + grp})
-    if turned_chunk is not None:
-        for dh in range(1, high_n):
-            signal(side_sem, turned_kv((high + dh) % high_n, outer))
-        if high_n > 1:
-            pl.semaphore_wait(side_sem, high_n - 1)
-        for i, (dh, dy) in enumerate(steps):
-            h, y = (high + dh) % high_n, (outer + dy) % outer_n
-            go(nturn.at[h * outer_n + y], aturn.at[i], turn_recv, turned_kv(h, y))
 
     for copy in small[1:]:
         copy.wait()
@@ -387,6 +379,15 @@
                 go(piece, piece, f_recv.at[c, i, j], at_grp(p))
         if c + 2 < chunks:
             direct(c + 2)
+
+    def send_turned():
+        for dh in range(1, high_n):
+            signal(side_sem, turned_kv((high + dh) % high_n, outer))
+        if high_n > 1:
+            pl.semaphore_wait(side_sem, high_n - 1)
+        for i, (dh, dy) in enumerate(steps):
+            h, y = (high + dh) % high_n, (outer + dy) % outer_n
+            go(nturn.at[h * outer_n + y], aturn.at[i], turn_recv, turned_kv(h, y))
 
     def receive_turned():
         xturn[...] = jnp.zeros_like(xturn)
@@ -482,15 +483,19 @@
             if c == 0:
                 mem_copy.wait()
             relay(c)
+            if c == 0 and turned_chunk is not None:
+                send_turned()
             for h in range(c, heads, 2) if c < 2 else ():
                 fold(h)
         if c == 1:
             receive_rows()
-            if turned_chunk is not None:
-                receive_turned()
+        if c == 3 and turned_chunk is not None:
+            receive_turned()
+        if c == 3:
+            finish(0)
         if 1 <= c <= chunks:
             partial(c - 1)
-        if c >= 3:
+        if c > 3:
             finish(c - 3)
     for copy in sends[-pool:]:
         copy.wait_send()

time: 32.6 us -> 32.4 us (level)
  no operation moved by 1% of the time
where the time goes in v4:
time: 32.4 us; the launch traced here: 32.2 us
  Pallas kernels  31.6 us (98%)
  between operations  0.65 us (2%)
    pallas_call x1, Pallas kernels, step(): pl.pallas_call(functools.partial(step_kernel, reduce_n, outer_n, inner_n,...  29 us
    pallas_call x1, Pallas kernels, step(): pl.pallas_call(write_kernel, out_shape=results, in_specs=[vmem] * len(res...  2.52 us

profile of v4, /device:TPU:0, one launch (start us, length us, event | category | flops | bytes accessed | tf_op | source)
XLA Modules:
  0.0 32.2 jit_solution(12549416953196387512)
XLA Ops:
  0.6 29.0 %step.1 = (bf16[10,3,1024]{2,1,0:T(4,128)(2,1)S(1)}, f32[10,4,128,256]{3,2,1,0:T(8,128)S(1)}, f32[10,4,128]{2,1,0:T(4,128)S(1)}, f32[4,10]{1,0:T(4,128)S(1)}) custom-call(bf16[10,3,1024]{2,1,0:T(4,128)(2,1)} %tok_ref.1, bf16[128,512]{1,0:T(8,128)(2,1)} %wq_ref.1, bf16[128,512]{1,0:T(8,128)(2,1)} %wk_ref.1, bf16[128,1024]{1,0:T(8,128)(2,1)} %wv_ref.1, ...), custom_call_target="tpu_custom_call" | custom-call | tf_op jit(solution)/shard_map/step/pallas_call | solution.py:575
  29.7 2.5 %write.1 = (bf16[10,3,1024]{2,1,0:T(4,128)(2,1)}, f32[10,4,128,256]{3,2,1,0:T(8,128)}, f32[10,4,128]{2,1,0:T(4,128)}, f32[4,10]{1,0:T(4,128)}) custom-call(bf16[10,3,1024]{2,1,0:T(4,128)(2,1)S(1)} %get-tuple-element.12.refs_0_, f32[10,4,128,256]{3,2,1,0:T(8,128)S(1)} %get-tuple-element.13.refs_1_, f32[10,4,128]{2,1,0:T(4,128)S(1)} %get-tuple-element.14.refs_2_, ...), custom_call_target="tpu_custom_call" | custom-call | tf_op jit(solution)/shard_map/write/pallas_call | solution.py:619
